TPU v7x, 512 devices: a whole 4x8x8 slice. The times are simulated.
512 devices in a mesh: tp: 32 (over z, x), dp: 16 (over y, core).
Axes of the slice: x: 4, y: 8, z: 8, core: 2. Of those that a mesh axis runs over, the one named last changes fastest.
Arguments:
- tokens: bfloat16 [256, 4096], P('dp', 'tp'), may hold values from -6 to 6
- norm_gain: float32 [2, 4096], replicated, may hold values from 0.1 to 1.9
- w_in: bfloat16 [2, 4096, 2048], P(None, 'dp', 'tp'), may hold values from -0.09375 to 0.09375
- w_gate: bfloat16 [2, 4096, 2048], P(None, 'dp', 'tp'), may hold values from -0.1875 to 0.1875
- decay_rate: float32 [2, 128, 64], P(None, 'tp'), may hold values from 0.05 to 2
- frequency: float32 [2, 128, 64], P(None, 'tp'), may hold values from -3 to 3
- log_step: float32 [2, 128], P(None, 'tp'), may hold values from -3 to 0
- map_re: float32 [2, 128, 16, 64], P(None, 'tp'), may hold values from -1.5 to 1.5
- map_im: float32 [2, 128, 16, 64], P(None, 'tp'), may hold values from -1.5 to 1.5
- read_re: float32 [2, 128, 16, 64], P(None, 'tp'), may hold values from -0.5 to 0.5
- read_im: float32 [2, 128, 16, 64], P(None, 'tp'), may hold values from -0.5 to 0.5
- skip_weight: float32 [2, 128, 16], P(None, 'tp'), may hold values from -4 to 4
- w_out: bfloat16 [2, 2048, 4096], P(None, 'dp', 'tp'), may hold values from -0.25 to 0.25
- state_re: float32 [2, 256, 128, 64], P(None, 'dp', 'tp'), may hold values from -6 to 6
- state_im: float32 [2, 256, 128, 64], P(None, 'dp', 'tp'), may hold values from -6 to 6
Outputs:
- hidden: bfloat16 [256, 4096], P('dp', 'tp')
- new_re: float32 [2, 256, 128, 64], P(None, 'dp', 'tp')
- new_im: float32 [2, 256, 128, 64], P(None, 'dp', 'tp')
All inputs are finite; a program needn't handle non-finite values.
Results may differ from a plain program's by a relative error of at most 0.01.
Values may be sent and summed in bfloat16 or wider, within the bound.
No kernel may reach another device: no remote copies, remote signals or barrier semaphores. Data moves between devices by JAX's collectives and lax.ppermute only.
A program may use at most 64 MiB of HBM per device.

v0:
```python
import jax
import jax.numpy as jnp
from jax import lax
from jax.sharding import PartitionSpec as P

EPSILON = 1e-06
HIGH = lax.Precision.HIGHEST


def from_everyone(array, axis):
    copies = jnp.broadcast_to(array, (lax.axis_size(axis), *array.shape))
    return lax.all_to_all(copies, axis, split_axis=0, concat_axis=0, tiled=True)


def laid_out(tiles, dim):
    dims = list(tiles.shape[1:])
    dims[dim] *= tiles.shape[0]
    return jnp.moveaxis(tiles, 0, dim).reshape(dims)


def gather_directly(array, axis, dim):
    tiles = from_everyone(array, axis)
    return laid_out(tiles, dim)


def in_one_piece(arrays, axis, dim, along):
    both = jnp.concatenate(arrays, axis=along)
    out, at, gathered = (lax.all_gather(both, axis, axis=dim, tiled=True), 0, [])
    for a in arrays:
        gathered.append(lax.slice_in_dim(out, at, at + a.shape[along], axis=along))
        at += a.shape[along]
    return tuple(gathered)


def state_update(
    inputs,
    old_re,
    old_im,
    decay_rate,
    frequency,
    log_step,
    map_re,
    map_im,
    read_re,
    read_im,
    skip_weight,
):
    lam_re = -decay_rate
    step_size = jnp.exp(log_step)[:, None]
    magnitude = jnp.exp(lam_re * step_size)
    decay_re = magnitude * jnp.cos(frequency * step_size)
    decay_im = magnitude * jnp.sin(frequency * step_size)
    modulus = lam_re * lam_re + frequency * frequency
    hold_re = ((decay_re - 1.0) * lam_re + decay_im * frequency) / modulus
    hold_im = (decay_im * lam_re - (decay_re - 1.0) * frequency) / modulus
    drive_re = hold_re[:, None, :] * map_re - hold_im[:, None, :] * map_im
    drive_im = hold_re[:, None, :] * map_im + hold_im[:, None, :] * map_re
    push_re = jnp.einsum("bgc,gcn->bgn", inputs, drive_re, precision=HIGH)
    push_im = jnp.einsum("bgc,gcn->bgn", inputs, drive_im, precision=HIGH)
    fresh_re = decay_re * old_re - decay_im * old_im + push_re
    fresh_im = decay_re * old_im + decay_im * old_re + push_im
    readout = (
        jnp.einsum("bgn,gcn->bgc", fresh_re, read_re, precision=HIGH)
        - jnp.einsum("bgn,gcn->bgc", fresh_im, read_im, precision=HIGH)
        + skip_weight * inputs
    )
    return (readout, fresh_re, fresh_im)


def local(
    tokens,
    norm_gain,
    w_in,
    w_gate,
    decay_rate,
    frequency,
    log_step,
    map_re,
    map_im,
    read_re,
    read_im,
    skip_weight,
    w_out,
    state_re,
    state_im,
):
    hidden = tokens
    seq_rows = tokens.shape[0]
    local_cols = w_in.shape[2]
    local_groups = decay_rate.shape[1]
    all_re = []
    all_im = []
    for layer in range(w_in.shape[0]):
        whole = gather_directly(hidden, "tp", 1)
        floats = whole.astype(jnp.float32)
        inv_scale = lax.rsqrt(jnp.mean(floats * floats, axis=-1, keepdims=True) + EPSILON)
        normed = (floats * inv_scale * norm_gain[layer]).astype(jnp.bfloat16)
        pieces = in_one_piece((w_in[layer], w_gate[layer]), "dp", 0, 1)
        drive_sum = jnp.dot(normed, pieces[0], preferred_element_type=jnp.float32)
        gate_sum = jnp.dot(normed, pieces[1], preferred_element_type=jnp.float32)
        projected = drive_sum.astype(jnp.bfloat16)
        gate = gate_sum.astype(jnp.bfloat16)
        inputs = projected.astype(jnp.float32).reshape(seq_rows, local_groups, -1)
        readout, fresh_re, fresh_im = state_update(
            inputs,
            state_re[layer],
            state_im[layer],
            decay_rate[layer],
            frequency[layer],
            log_step[layer],
            map_re[layer],
            map_im[layer],
            read_re[layer],
            read_im[layer],
            skip_weight[layer],
        )
        activated = jax.nn.gelu(readout.reshape(seq_rows, local_cols))
        mixer = (activated * jax.nn.sigmoid(gate.astype(jnp.float32))).astype(jnp.bfloat16)
        full_rows = gather_directly(mixer, "tp", 1)
        mixed = jnp.dot(
            full_rows,
            lax.all_gather(w_out[layer], "dp", axis=0, tiled=True),
            preferred_element_type=jnp.float32,
        )
        hidden = (hidden.astype(jnp.float32) + mixed).astype(jnp.bfloat16)
        all_re.append(fresh_re)
        all_im.append(fresh_im)
    return (hidden, jnp.stack(all_re), jnp.stack(all_im))


def solution(mesh):
    return jax.shard_map(
        local,
        mesh=mesh,
        in_specs=(
            P("dp", "tp"),
            P(),
            P(None, "dp", "tp"),
            P(None, "dp", "tp"),
            P(None, "tp", None),
            P(None, "tp", None),
            P(None, "tp"),
            P(None, "tp", None, None),
            P(None, "tp", None, None),
            P(None, "tp", None, None),
            P(None, "tp", None, None),
            P(None, "tp", None),
            P(None, "dp", "tp"),
            P(None, "dp", "tp", None),
            P(None, "dp", "tp", None),
        ),
        out_specs=(P("dp", "tp"), P(None, "dp", "tp", None), P(None, "dp", "tp", None)),
        check_vma=False,
    )
```

profile of v0, /device:TPU:8, one launch (start us, length us, event | category | flops | bytes accessed | tf_op | source)
XLA Modules:
  0.0 148.4 jit_solution(1583821423735559264)
XLA Ops:
  7.2 0.8 slice_bitcast_fusion.2
  8.0 0.6 pad_maximum_fusion
  8.7 0.7 copy-done.8
  9.4 0.7 broadcast_in_dim.8
  10.0 13.2 %all-to-all-start = ((bf16[32,16,128]{2,1,0:T(8,128)(2,1)}), bf16[32,16,128]{2,1,0:T(8,128)(2,1)S(1)}, u32[]{:S(2)}, u32[]{:S(2)}) async-start(bf16[32,16,128]{2,1,0:T(8,128)(2,1)} %broadcast_in_dim.8), calls=%async_computation | async-start | bytes 262144 | tf_op jit(solution)/shard_map/all_to_all | solution.py:12
  23.2 0.6 pad_maximum_fusion.1
  23.9 0.6 copy-done.12
  24.9 0.5 copy-done.3
  25.6 0.7 copy-done.4
  26.3 7.4 %all-to-all-done = bf16[32,16,128]{2,1,0:T(8,128)(2,1)S(1)} async-done(((bf16[32,16,128]{2,1,0:T(8,128)(2,1)}), bf16[32,16,128]{2,1,0:T(8,128)(2,1)S(1)}, u32[]{:S(2)}, u32[]{:S(2)}) %all-to-all-start) | async-done | bytes 131104 | tf_op jit(solution)/shard_map/all_to_all | solution.py:12
  33.8 21.3 %all-gather.5.cloned.1.call-done = bf16[4096,128]{0,1:T(8,128)(2,1)} async-done(((bf16[256,128]{0,1:T(8,128)(2,1)}), bf16[4096,128]{0,1:T(8,128)(2,1)}) %all-gather.5.cloned.1.call-update) | async-done | bytes 1048592 | tf_op jit(solution)/shard_map/all_gather | solution.py:28
  55.1 1.4 convolution_convert_fusion.3
  56.7 0.7 copy-done.2
  57.8 0.7 copy-done.6
  58.7 1.4 fusion.21
  60.1 0.8 reshape.326
  60.9 10.1 %all-to-all-start.1 = ((bf16[32,2,512]{2,1,0:T(2,128)(2,1)}), bf16[32,2,512]{2,1,0:T(2,128)(2,1)S(1)}, u32[]{:S(2)}, u32[]{:S(2)}) async-start(bf16[32,2,512]{2,1,0:T(2,128)(2,1)} %reshape.326), calls=%async_computation.1 | async-start | bytes 131072 | tf_op jit(solution)/shard_map/all_to_all | solution.py:12
  71.0 16.1 %all-gather = bf16[1,2048,128]{2,1,0:T(8,128)(2,1)S(1)} all-gather(bf16[1,128,128]{2,1,0:T(8,128)(2,1)S(1)} %get-tuple-element.13), channel_id=2, replica_groups=mesh['tp'=32,'dp'=16] {'dp'}, dimensions={1}, use_global_device_ids=true | all-gather | bytes 557056 | tf_op jit(solution)/shard_map/all_gather | solution.py:122
  87.3 0.2 reshape.315
  87.5 0.2 fusion.22
  87.7 0.7 broadcast_in_dim.10
  88.3 10.2 %all-to-all-start.2 = ((bf16[32,16,128]{2,1,0:T(8,128)(2,1)}), bf16[32,16,128]{2,1,0:T(8,128)(2,1)S(1)}, u32[]{:S(2)}, u32[]{:S(2)}) async-start(bf16[32,16,128]{2,1,0:T(8,128)(2,1)} %broadcast_in_dim.10), calls=%async_computation.2 | async-start | bytes 262144 | tf_op jit(solution)/shard_map/all_to_all | solution.py:12
  98.6 18.5 %all-gather.1 = bf16[1,2048,128]{2,1,0:T(8,128)(2,1)S(1)} all-gather(bf16[1,128,128]{2,1,0:T(8,128)(2,1)S(1)} %get-tuple-element.12), channel_id=3, replica_groups=mesh['tp'=32,'dp'=16] {'dp'}, dimensions={1}, use_global_device_ids=true | all-gather | bytes 557056 | tf_op jit(solution)/shard_map/all_gather | solution.py:122
  117.3 1.4 convolution_convert_fusion.1
  119.6 0.3 fusion.14
  119.9 0.8 reshape.328
  120.7 9.8 %all-to-all-start.3 = ((bf16[32,2,512]{2,1,0:T(2,128)(2,1)}), bf16[32,2,512]{2,1,0:T(2,128)(2,1)S(1)}, u32[]{:S(2)}, u32[]{:S(2)}) async-start(bf16[32,2,512]{2,1,0:T(2,128)(2,1)} %reshape.328), calls=%async_computation.3 | async-start | bytes 131072 | tf_op jit(solution)/shard_map/all_to_all | solution.py:12
  130.5 0.7 copy.62
  131.1 0.7 copy.61
  131.8 8.6 %all-to-all-done.3 = bf16[32,2,512]{2,1,0:T(2,128)(2,1)S(1)} async-done(((bf16[32,2,512]{2,1,0:T(2,128)(2,1)}), bf16[32,2,512]{2,1,0:T(2,128)(2,1)S(1)}, u32[]{:S(2)}, u32[]{:S(2)}) %all-to-all-start.3) | async-done | bytes 65568 | tf_op jit(solution)/shard_map/all_to_all | solution.py:12
  140.6 0.2 reshape.319
  140.8 0.8 fusion.23
  (62 shorter events, 3.1 us)
Async XLA Ops:
  7.2 47.9 %all-gather.5.cloned.1.call-start = ((), (), s32[]{:S(2)}) async-start(), calls=%async_computation.4 | async-start | bytes 1114112 | tf_op jit(solution)/shard_map/all_gather | solution.py:28
  8.7 0.7 copy-start.8
  10.0 23.6 %all-to-all-start = ((bf16[32,16,128]{2,1,0:T(8,128)(2,1)}), bf16[32,16,128]{2,1,0:T(8,128)(2,1)S(1)}, u32[]{:S(2)}, u32[]{:S(2)}) async-start(bf16[32,16,128]{2,1,0:T(8,128)(2,1)} %broadcast_in_dim.8), calls=%async_computation | async-start | bytes 262144 | tf_op jit(solution)/shard_map/all_to_all | solution.py:12
  23.2 94.1 %all-gather.7.cloned.1.call-start = ((), (), s32[]{:S(2)}) async-start(), calls=%async_computation.5 | async-start | bytes 1114112 | tf_op jit(solution)/shard_map/all_gather | solution.py:28
  23.9 0.7 copy-start.12
  23.9 0.7 copy-start.9
  23.9 0.7 copy-start.10
  23.9 1.0 copy-start.7
  24.6 0.8 copy-start.3
  24.9 0.7 copy-start.11
  25.4 0.8 copy-start.4
  25.4 0.9 copy-start.5
  55.1 1.5 copy-start
  55.1 1.5 copy-start.1
  56.6 0.8 copy-start.2
  57.6 0.8 copy-start.6
  60.9 26.2 %all-to-all-start.1 = ((bf16[32,2,512]{2,1,0:T(2,128)(2,1)}), bf16[32,2,512]{2,1,0:T(2,128)(2,1)S(1)}, u32[]{:S(2)}, u32[]{:S(2)}) async-start(bf16[32,2,512]{2,1,0:T(2,128)(2,1)} %reshape.326), calls=%async_computation.1 | async-start | bytes 131072 | tf_op jit(solution)/shard_map/all_to_all | solution.py:12
  88.3 28.7 %all-to-all-start.2 = ((bf16[32,16,128]{2,1,0:T(8,128)(2,1)}), bf16[32,16,128]{2,1,0:T(8,128)(2,1)S(1)}, u32[]{:S(2)}, u32[]{:S(2)}) async-start(bf16[32,16,128]{2,1,0:T(8,128)(2,1)} %broadcast_in_dim.10), calls=%async_computation.2 | async-start | bytes 262144 | tf_op jit(solution)/shard_map/all_to_all | solution.py:12
  117.3 2.3 %copy-start.13 = (bf16[4096,128]{0,1:T(8,128)(2,1)S(1)}, bf16[4096,128]{0,1:T(8,128)(2,1)}, u32[]{:S(2)}) copy-start(bf16[4096,128]{0,1:T(8,128)(2,1)} %all-gather.7.cloned.1.call-done) | copy-start | bytes 3145732
  120.7 19.8 %all-to-all-start.3 = ((bf16[32,2,512]{2,1,0:T(2,128)(2,1)}), bf16[32,2,512]{2,1,0:T(2,128)(2,1)S(1)}, u32[]{:S(2)}, u32[]{:S(2)}) async-start(bf16[32,2,512]{2,1,0:T(2,128)(2,1)} %reshape.328), calls=%async_computation.3 | async-start | bytes 131072 | tf_op jit(solution)/shard_map/all_to_all | solution.py:12
Sparse Core Ops, SparseCore 0:
  10.6 44.4 all-gather.4
  57.7 39.4 all-gather.6
where the time goes:
time: 149 us; the launch traced here: 148 us
  starting transfers between devices  43.4 us (29%)
  waiting for transfers between devices  37.4 us (25%)
  blocking collectives  34.5 us (23%)
  between operations  14.3 us (10%)
  local copies, waits for them, and re-layouts  10.2 us (7%)
  matrix products  6.73 us (5%)
  other arithmetic  1.84 us (1%)
    all_to_all x4, starting transfers between devices, from_everyone(): return lax.all_to_all(copies, axis, split_axis=0, concat_axis=0, tiled=True)  43.3 us
    all_gather x2, blocking collectives, local(): lax.all_gather(w_out[layer], 'dp', axis=0, tiled=True)  34.5 us
    all_gather x2, waiting for transfers between devices, in_one_piece(): lax.all_gather(both, axis, axis=dim, tiled=True)  21.3 us
    all_to_all x4, waiting for transfers between devices, from_everyone(): return lax.all_to_all(copies, axis, split_axis=0, concat_axis=0, tiled=True)  16 us
    unnamed x34, local copies, waits for them, and re-layouts  7.18 us
  transfers between devices with their start and end apart: 6, of which 3 were waited for; matrix products, arithmetic and copies ran while one was open for 6% of the time, Pallas kernels for 0%

commit v1 on v0

--- a/solution.py
+++ b/solution.py
@@ -5,6 +5,28 @@
 
 EPSILON = 1e-06
 HIGH = lax.Precision.HIGHEST
+
+
+def joined_along(blocks, dim):
+    blocks = jnp.moveaxis(blocks, 0, dim)
+    shape = blocks.shape
+    return blocks.reshape(*shape[:dim], shape[dim] * shape[dim + 1], *shape[dim + 2 :])
+
+
+def gather_around(array, axis, dim):
+    length = lax.axis_size(axis)
+    pairs = [(i, (i + 1) % length) for i in range(length)]
+    back = [(b, a) for a, b in pairs]
+    lower, upper = ([], [])
+    for step in range(length - 1):
+        if step % 2 == 0:
+            lower.append(lax.ppermute(lower[-1] if lower else array, axis, pairs))
+        else:
+            upper.append(lax.ppermute(upper[-1] if upper else array, axis, back))
+    blocks = jnp.stack([*lower[::-1], array, *upper])
+    shift = lax.axis_index(axis) - len(lower)
+    blocks = blocks[(jnp.arange(length) - shift) % length]
+    return joined_along(blocks, dim)
 
 
 def from_everyone(array, axis):
@@ -118,9 +140,7 @@
         mixer = (activated * jax.nn.sigmoid(gate.astype(jnp.float32))).astype(jnp.bfloat16)
         full_rows = gather_directly(mixer, "tp", 1)
         mixed = jnp.dot(
-            full_rows,
-            lax.all_gather(w_out[layer], "dp", axis=0, tiled=True),
-            preferred_element_type=jnp.float32,
+            full_rows, gather_around(w_out[layer], "dp", 0), preferred_element_type=jnp.float32
         )
         hidden = (hidden.astype(jnp.float32) + mixed).astype(jnp.bfloat16)
         all_re.append(fresh_re)

time: 149 us -> 132 us (0.89)
  the two profiles are of different devices: /device:TPU:8 before, /device:TPU:32 now
where the time goes in v1:
time: 132 us; the launch traced here: 131 us
  starting transfers between devices  56.7 us (43%)
  waiting for transfers between devices  40 us (30%)
  between operations  14.6 us (11%)
  local copies, waits for them, and re-layouts  11.4 us (9%)
  matrix products  6.74 us (5%)
  other arithmetic  1.86 us (1%)
    all_to_all x4, starting transfers between devices, from_everyone(): return lax.all_to_all(copies, axis, split_axis=0, concat_axis=0, tiled=True)  30.2 us
    all_to_all x4, waiting for transfers between devices, from_everyone(): return lax.all_to_all(copies, axis, split_axis=0, concat_axis=0, tiled=True)  28.5 us
    ppermute x14, starting transfers between devices, gather_around(): upper.append(lax.ppermute(upper[-1] if upper else array, axis, back))  26.4 us
    ppermute x16, waiting for transfers between devices, gather_around(): lower.append(lax.ppermute(lower[-1] if lower else array, axis, pairs))  9.53 us
    unnamed x63, local copies, waits for them, and re-layouts  7 us
    dot_general x2, matrix products, local(): drive_sum = jnp.dot(normed, pieces[0], preferred_element_type=jnp.float32)  2.8 us
  transfers between devices with their start and end apart: 36, of which 17 were waited for; matrix products, arithmetic and copies ran while one was open for 8% of the time, Pallas kernels for 0%

profile of v1, /device:TPU:32, one launch (start us, length us, event | category | flops | bytes accessed | tf_op | source)
XLA Modules:
  0.0 131.3 jit_solution(6057429354853954351)
XLA Ops:
  7.2 0.8 slice_bitcast_fusion.2
  8.7 0.8 copy-done
  9.5 2.9 %collective-permute-start.8 = (bf16[128,128]{1,0:T(8,128)(2,1)S(1)}, bf16[128,128]{1,0:T(8,128)(2,1)S(1)}, u32[]{:S(2)}, u32[]{:S(2)}) collective-permute-start(bf16[128,128]{1,0:T(8,128)(2,1)S(1)} %get-tuple-element.15), channel_id=1, source_target_pairs={{1,0},{2,1},{3,2},{4,3},{5,4},{6,5},{7,6},{8,7},{9,8},{10,9},{11,1... | collective-permute-start | bytes 98312 | tf_op jit(solution)/shard_map/ppermute | solution.py:25
  12.5 3.0 %collective-permute-start.23 = (bf16[128,128]{1,0:T(8,128)(2,1)S(1)}, bf16[128,128]{1,0:T(8,128)(2,1)S(1)}, u32[]{:S(2)}, u32[]{:S(2)}) collective-permute-start(bf16[128,128]{1,0:T(8,128)(2,1)S(1)} %get-tuple-element.14), channel_id=1, source_target_pairs={{1,0},{2,1},{3,2},{4,3},{5,4},{6,5},{7,6},{8,7},{9,8},{10,9},{11,1... | collective-permute-start | bytes 98312 | tf_op jit(solution)/shard_map/ppermute | solution.py:25
  16.1 13.2 %all-to-all-start = ((bf16[32,16,128]{2,1,0:T(8,128)(2,1)}), bf16[32,16,128]{2,1,0:T(8,128)(2,1)S(1)}, u32[]{:S(2)}, u32[]{:S(2)}) async-start(bf16[32,16,128]{2,1,0:T(8,128)(2,1)} %broadcast_in_dim.8), calls=%async_computation | async-start | bytes 262144 | tf_op jit(solution)/shard_map/all_to_all | solution.py:34
  30.1 0.7 copy-done.4
  31.5 2.4 %collective-permute-start.9 = (bf16[128,128]{1,0:T(8,128)(2,1)S(1)}, bf16[128,128]{1,0:T(8,128)(2,1)S(1)}, u32[]{:S(2)}, u32[]{:S(2)}) collective-permute-start(bf16[128,128]{1,0:T(8,128)(2,1)S(1)} %collective-permute-done.8), channel_id=1, source_target_pairs={{1,0},{2,1},{3,2},{4,3},{5,4},{6,5},{7,6},{8,7},{9,8},{10,9},{11,1... | collective-permute-start | bytes 98312 | tf_op jit(solution)/shard_map/ppermute | solution.py:25
  34.4 1.0 collective-permute-done.1
  36.1 3.0 %collective-permute-start.10 = (bf16[128,128]{1,0:T(8,128)(2,1)S(1)}, bf16[128,128]{1,0:T(8,128)(2,1)S(1)}, u32[]{:S(2)}, u32[]{:S(2)}) collective-permute-start(bf16[128,128]{1,0:T(8,128)(2,1)S(1)} %collective-permute-done.9), channel_id=1, source_target_pairs={{1,0},{2,1},{3,2},{4,3},{5,4},{6,5},{7,6},{8,7},{9,8},{10,9},{11,1... | collective-permute-start | bytes 98312 | tf_op jit(solution)/shard_map/ppermute | solution.py:25
  40.2 0.8 collective-permute-done.17
  41.2 3.0 %collective-permute-start.11 = (bf16[128,128]{1,0:T(8,128)(2,1)S(1)}, bf16[128,128]{1,0:T(8,128)(2,1)S(1)}, u32[]{:S(2)}, u32[]{:S(2)}) collective-permute-start(bf16[128,128]{1,0:T(8,128)(2,1)S(1)} %collective-permute-done.10), channel_id=1, source_target_pairs={{1,0},{2,1},{3,2},{4,3},{5,4},{6,5},{7,6},{8,7},{9,8},{10,9},{11,1... | collective-permute-start | bytes 98312 | tf_op jit(solution)/shard_map/ppermute | solution.py:25
  44.8 0.8 collective-permute-done.18
  45.9 3.5 %collective-permute-start.12 = (bf16[128,128]{1,0:T(8,128)(2,1)S(1)}, bf16[128,128]{1,0:T(8,128)(2,1)S(1)}, u32[]{:S(2)}, u32[]{:S(2)}) collective-permute-start(bf16[128,128]{1,0:T(8,128)(2,1)S(1)} %collective-permute-done.11), channel_id=1, source_target_pairs={{1,0},{2,1},{3,2},{4,3},{5,4},{6,5},{7,6},{8,7},{9,8},{10,9},{11,1... | collective-permute-start | bytes 98312 | tf_op jit(solution)/shard_map/ppermute | solution.py:25
  50.2 0.9 collective-permute-done.12
  51.0 3.0 %collective-permute-start.13 = (bf16[128,128]{1,0:T(8,128)(2,1)S(1)}, bf16[128,128]{1,0:T(8,128)(2,1)S(1)}, u32[]{:S(2)}, u32[]{:S(2)}) collective-permute-start(bf16[128,128]{1,0:T(8,128)(2,1)S(1)} %collective-permute-done.12), channel_id=1, source_target_pairs={{1,0},{2,1},{3,2},{4,3},{5,4},{6,5},{7,6},{8,7},{9,8},{10,9},{11,1... | collective-permute-start | bytes 98312 | tf_op jit(solution)/shard_map/ppermute | solution.py:25
  55.6 3.0 %collective-permute-start.14 = (bf16[128,128]{1,0:T(8,128)(2,1)S(1)}, bf16[128,128]{1,0:T(8,128)(2,1)S(1)}, u32[]{:S(2)}, u32[]{:S(2)}) collective-permute-start(bf16[128,128]{1,0:T(8,128)(2,1)S(1)} %collective-permute-done.13), channel_id=1, source_target_pairs={{1,0},{2,1},{3,2},{4,3},{5,4},{6,5},{7,6},{8,7},{9,8},{10,9},{11,1... | collective-permute-start | bytes 98312 | tf_op jit(solution)/shard_map/ppermute | solution.py:25
  59.6 4.0 %collective-permute-done.7 = bf16[128,128]{1,0:T(8,128)(2,1)S(1)} collective-permute-done((bf16[128,128]{1,0:T(8,128)(2,1)S(1)}, bf16[128,128]{1,0:T(8,128)(2,1)S(1)}, u32[]{:S(2)}, u32[]{:S(2)}) %collective-permute-start.7) | collective-permute-done | bytes 32800 | tf_op jit(solution)/shard_map/ppermute | solution.py:23
  65.0 1.4 %convolution_convert_fusion.3 = bf16[16,64]{1,0:T(8,128)(2,1)S(1)} fusion(bf16[4096,128]{0,1:T(8,128)(2,1)} %all-gather.3.cloned.1.call-done, f32[4096]{0:T(1024)S(1)} %bitcast.358, f32[16]{0:T(128)S(1)} %add_rsqrt_fusion.1, bf16[32,16,128]{2,1,0:T(8,128)(2,1)S(1)} %all-to-all-done), kind=kOutput, calls=%fused_computation.35 | convolution fusion | flops 8651776 | bytes 673856 | tf_op jit(solution)/shard_map/dot_general | solution.py:121
  66.7 0.7 copy-done.3
  67.7 0.7 copy-done.6
  68.7 1.4 %fusion.21 = bf16[16,64]{1,0:T(8,128)(2,1)S(1)} fusion(bf16[4096,128]{0,1:T(8,128)(2,1)} %all-gather.3.cloned.1.call-done, f32[16,64]{1,0:T(8,128)S(1)} %reshape.369, f32[4096]{0:T(1024)S(1)} %bitcast.359, f32[16]{0:T(128)S(1)} %add_rsqrt_fusion.1, bf16[32,16,128]{2,1,0:T(8,128)(2,1)S(1)} %all-to-all-done), kind=kOutput, calls=%fused_computation.34 | convolution fusion | flops 8666112 | bytes 677952 | tf_op jit(solution)/shard_map/dot_general | solution.py:122
  70.1 0.8 reshape.397
  70.8 9.3 %all-to-all-start.1 = ((bf16[32,2,512]{2,1,0:T(2,128)(2,1)}), bf16[32,2,512]{2,1,0:T(2,128)(2,1)S(1)}, u32[]{:S(2)}, u32[]{:S(2)}) async-start(bf16[32,2,512]{2,1,0:T(2,128)(2,1)} %reshape.397), calls=%async_computation.1 | async-start | bytes 131072 | tf_op jit(solution)/shard_map/all_to_all | solution.py:34
  80.2 10.0 %all-to-all-done.1 = bf16[32,2,512]{2,1,0:T(2,128)(2,1)S(1)} async-done(((bf16[32,2,512]{2,1,0:T(2,128)(2,1)}), bf16[32,2,512]{2,1,0:T(2,128)(2,1)S(1)}, u32[]{:S(2)}, u32[]{:S(2)}) %all-to-all-start.1) | async-done | bytes 65568 | tf_op jit(solution)/shard_map/all_to_all | solution.py:34
  90.7 0.7 broadcast_in_dim.10
  91.4 3.9 %all-to-all-start.2 = ((bf16[32,16,128]{2,1,0:T(8,128)(2,1)}), bf16[32,16,128]{2,1,0:T(8,128)(2,1)S(1)}, u32[]{:S(2)}, u32[]{:S(2)}) async-start(bf16[32,16,128]{2,1,0:T(8,128)(2,1)} %broadcast_in_dim.10), calls=%async_computation.2 | async-start | bytes 262144 | tf_op jit(solution)/shard_map/all_to_all | solution.py:34
  96.0 9.9 %all-to-all-done.2 = bf16[32,16,128]{2,1,0:T(8,128)(2,1)S(1)} async-done(((bf16[32,16,128]{2,1,0:T(8,128)(2,1)}), bf16[32,16,128]{2,1,0:T(8,128)(2,1)S(1)}, u32[]{:S(2)}, u32[]{:S(2)}) %all-to-all-start.2) | async-done | bytes 131104 | tf_op jit(solution)/shard_map/all_to_all | solution.py:34
  106.0 1.4 %convolution_convert_fusion.1 = bf16[16,64]{1,0:T(8,128)(2,1)S(1)} fusion(bf16[4096,128]{0,1:T(8,128)(2,1)} %all-gather.5.cloned.1.call-done, f32[4096]{0:T(1024)S(1)} %bitcast.356, f32[16]{0:T(128)S(1)} %add_rsqrt_fusion, bf16[32,16,128]{2,1,0:T(8,128)(2,1)S(1)} %all-to-all-done.2), kind=kOutput, calls=%fused_computation.26 | convolution fusion | flops 8651776 | bytes 673856 | tf_op jit(solution)/shard_map/dot_general | solution.py:121
  108.7 0.7 reshape.399
  109.4 3.8 %all-to-all-start.3 = ((bf16[32,2,512]{2,1,0:T(2,128)(2,1)}), bf16[32,2,512]{2,1,0:T(2,128)(2,1)S(1)}, u32[]{:S(2)}, u32[]{:S(2)}) async-start(bf16[32,2,512]{2,1,0:T(2,128)(2,1)} %reshape.399), calls=%async_computation.3 | async-start | bytes 131072 | tf_op jit(solution)/shard_map/all_to_all | solution.py:34
  114.6 8.7 %all-to-all-done.3 = bf16[32,2,512]{2,1,0:T(2,128)(2,1)S(1)} async-done(((bf16[32,2,512]{2,1,0:T(2,128)(2,1)}), bf16[32,2,512]{2,1,0:T(2,128)(2,1)S(1)}, u32[]{:S(2)}, u32[]{:S(2)}) %all-to-all-start.3) | async-done | bytes 65568 | tf_op jit(solution)/shard_map/all_to_all | solution.py:34
  123.7 0.8 fusion.23
  (155 shorter events, 15.9 us)
Async XLA Ops:
  7.2 57.8 %all-gather.3.cloned.1.call-start = ((), (), s32[]{:S(2)}) async-start(), calls=%async_computation.4 | async-start | bytes 1114112 | tf_op jit(solution)/shard_map/all_gather | solution.py:50
  9.5 21.4 %collective-permute-start = (bf16[128,128]{1,0:T(8,128)(2,1)S(1)}, bf16[128,128]{1,0:T(8,128)(2,1)S(1)}, u32[]{:S(2)}, u32[]{:S(2)}) collective-permute-start(bf16[128,128]{1,0:T(8,128)(2,1)S(1)} %get-tuple-element.15), channel_id=1, source_target_pairs={{0,1},{1,2},{2,3},{3,4},{4,5},{5,6},{6,7},{7,8},{8,9},{9,10},{10,1... | collective-permute-start | bytes 98312 | tf_op jit(solution)/shard_map/ppermute | solution.py:23
  9.5 22.0 %collective-permute-start.8 = (bf16[128,128]{1,0:T(8,128)(2,1)S(1)}, bf16[128,128]{1,0:T(8,128)(2,1)S(1)}, u32[]{:S(2)}, u32[]{:S(2)}) collective-permute-start(bf16[128,128]{1,0:T(8,128)(2,1)S(1)} %get-tuple-element.15), channel_id=1, source_target_pairs={{1,0},{2,1},{3,2},{4,3},{5,4},{6,5},{7,6},{8,7},{9,8},{10,9},{11,1... | collective-permute-start | bytes 98312 | tf_op jit(solution)/shard_map/ppermute | solution.py:25
  12.5 18.4 %collective-permute-start.15 = (bf16[128,128]{1,0:T(8,128)(2,1)S(1)}, bf16[128,128]{1,0:T(8,128)(2,1)S(1)}, u32[]{:S(2)}, u32[]{:S(2)}) collective-permute-start(bf16[128,128]{1,0:T(8,128)(2,1)S(1)} %get-tuple-element.14), channel_id=1, source_target_pairs={{0,1},{1,2},{2,3},{3,4},{4,5},{5,6},{6,7},{7,8},{8,9},{9,10},{10,1... | collective-permute-start | bytes 98312 | tf_op jit(solution)/shard_map/ppermute | solution.py:23
  12.5 21.5 %collective-permute-start.23 = (bf16[128,128]{1,0:T(8,128)(2,1)S(1)}, bf16[128,128]{1,0:T(8,128)(2,1)S(1)}, u32[]{:S(2)}, u32[]{:S(2)}) collective-permute-start(bf16[128,128]{1,0:T(8,128)(2,1)S(1)} %get-tuple-element.14), channel_id=1, source_target_pairs={{1,0},{2,1},{3,2},{4,3},{5,4},{6,5},{7,6},{8,7},{9,8},{10,9},{11,1... | collective-permute-start | bytes 98312 | tf_op jit(solution)/shard_map/ppermute | solution.py:25
  16.1 43.4 %all-to-all-start = ((bf16[32,16,128]{2,1,0:T(8,128)(2,1)}), bf16[32,16,128]{2,1,0:T(8,128)(2,1)S(1)}, u32[]{:S(2)}, u32[]{:S(2)}) async-start(bf16[32,16,128]{2,1,0:T(8,128)(2,1)} %broadcast_in_dim.8), calls=%async_computation | async-start | bytes 262144 | tf_op jit(solution)/shard_map/all_to_all | solution.py:34
  29.3 76.7 %all-gather.5.cloned.1.call-start = ((), (), s32[]{:S(2)}) async-start(), calls=%async_computation.5 | async-start | bytes 1114112 | tf_op jit(solution)/shard_map/all_gather | solution.py:50
  30.9 4.6 %collective-permute-start.1 = (bf16[128,128]{1,0:T(8,128)(2,1)S(1)}, bf16[128,128]{1,0:T(8,128)(2,1)S(1)}, u32[]{:S(2)}, u32[]{:S(2)}) collective-permute-start(bf16[128,128]{1,0:T(8,128)(2,1)S(1)} %collective-permute-done), channel_id=1, source_target_pairs={{0,1},{1,2},{2,3},{3,4},{4,5},{5,6},{6,7},{7,8},{8,9},{9,10},{10,1... | collective-permute-start | bytes 98312 | tf_op jit(solution)/shard_map/ppermute | solution.py:23
  30.9 5.0 %collective-permute-start.16 = (bf16[128,128]{1,0:T(8,128)(2,1)S(1)}, bf16[128,128]{1,0:T(8,128)(2,1)S(1)}, u32[]{:S(2)}, u32[]{:S(2)}) collective-permute-start(bf16[128,128]{1,0:T(8,128)(2,1)S(1)} %collective-permute-done.15), channel_id=1, source_target_pairs={{0,1},{1,2},{2,3},{3,4},{4,5},{5,6},{6,7},{7,8},{8,9},{9,10},{10,1... | collective-permute-start | bytes 98312 | tf_op jit(solution)/shard_map/ppermute | solution.py:23
  31.5 4.6 %collective-permute-start.9 = (bf16[128,128]{1,0:T(8,128)(2,1)S(1)}, bf16[128,128]{1,0:T(8,128)(2,1)S(1)}, u32[]{:S(2)}, u32[]{:S(2)}) collective-permute-start(bf16[128,128]{1,0:T(8,128)(2,1)S(1)} %collective-permute-done.8), channel_id=1, source_target_pairs={{1,0},{2,1},{3,2},{4,3},{5,4},{6,5},{7,6},{8,7},{9,8},{10,9},{11,1... | collective-permute-start | bytes 98312 | tf_op jit(solution)/shard_map/ppermute | solution.py:25
  33.9 5.1 %collective-permute-start.24 = (bf16[128,128]{1,0:T(8,128)(2,1)S(1)}, bf16[128,128]{1,0:T(8,128)(2,1)S(1)}, u32[]{:S(2)}, u32[]{:S(2)}) collective-permute-start(bf16[128,128]{1,0:T(8,128)(2,1)S(1)} %collective-permute-done.23), channel_id=1, source_target_pairs={{1,0},{2,1},{3,2},{4,3},{5,4},{6,5},{7,6},{8,7},{9,8},{10,9},{11,1... | collective-permute-start | bytes 98312 | tf_op jit(solution)/shard_map/ppermute | solution.py:25
  35.5 4.8 %collective-permute-start.2 = (bf16[128,128]{1,0:T(8,128)(2,1)S(1)}, bf16[128,128]{1,0:T(8,128)(2,1)S(1)}, u32[]{:S(2)}, u32[]{:S(2)}) collective-permute-start(bf16[128,128]{1,0:T(8,128)(2,1)S(1)} %collective-permute-done.1), channel_id=1, source_target_pairs={{0,1},{1,2},{2,3},{3,4},{4,5},{5,6},{6,7},{7,8},{8,9},{9,10},{10,1... | collective-permute-start | bytes 98312 | tf_op jit(solution)/shard_map/ppermute | solution.py:23
  35.9 5.1 %collective-permute-start.17 = (bf16[128,128]{1,0:T(8,128)(2,1)S(1)}, bf16[128,128]{1,0:T(8,128)(2,1)S(1)}, u32[]{:S(2)}, u32[]{:S(2)}) collective-permute-start(bf16[128,128]{1,0:T(8,128)(2,1)S(1)} %collective-permute-done.16), channel_id=1, source_target_pairs={{0,1},{1,2},{2,3},{3,4},{4,5},{5,6},{6,7},{7,8},{8,9},{9,10},{10,1... | collective-permute-start | bytes 98312 | tf_op jit(solution)/shard_map/ppermute | solution.py:23
  36.1 5.1 %collective-permute-start.10 = (bf16[128,128]{1,0:T(8,128)(2,1)S(1)}, bf16[128,128]{1,0:T(8,128)(2,1)S(1)}, u32[]{:S(2)}, u32[]{:S(2)}) collective-permute-start(bf16[128,128]{1,0:T(8,128)(2,1)S(1)} %collective-permute-done.9), channel_id=1, source_target_pairs={{1,0},{2,1},{3,2},{4,3},{5,4},{6,5},{7,6},{8,7},{9,8},{10,9},{11,1... | collective-permute-start | bytes 98312 | tf_op jit(solution)/shard_map/ppermute | solution.py:25
  39.1 5.1 %collective-permute-start.25 = (bf16[128,128]{1,0:T(8,128)(2,1)S(1)}, bf16[128,128]{1,0:T(8,128)(2,1)S(1)}, u32[]{:S(2)}, u32[]{:S(2)}) collective-permute-start(bf16[128,128]{1,0:T(8,128)(2,1)S(1)} %collective-permute-done.24), channel_id=1, source_target_pairs={{1,0},{2,1},{3,2},{4,3},{5,4},{6,5},{7,6},{8,7},{9,8},{10,9},{11,1... | collective-permute-start | bytes 98312 | tf_op jit(solution)/shard_map/ppermute | solution.py:25
  40.2 4.6 %collective-permute-start.3 = (bf16[128,128]{1,0:T(8,128)(2,1)S(1)}, bf16[128,128]{1,0:T(8,128)(2,1)S(1)}, u32[]{:S(2)}, u32[]{:S(2)}) collective-permute-start(bf16[128,128]{1,0:T(8,128)(2,1)S(1)} %collective-permute-done.2), channel_id=1, source_target_pairs={{0,1},{1,2},{2,3},{3,4},{4,5},{5,6},{6,7},{7,8},{8,9},{9,10},{10,1... | collective-permute-start | bytes 98312 | tf_op jit(solution)/shard_map/ppermute | solution.py:23
  41.1 4.6 %collective-permute-start.18 = (bf16[128,128]{1,0:T(8,128)(2,1)S(1)}, bf16[128,128]{1,0:T(8,128)(2,1)S(1)}, u32[]{:S(2)}, u32[]{:S(2)}) collective-permute-start(bf16[128,128]{1,0:T(8,128)(2,1)S(1)} %collective-permute-done.17), channel_id=1, source_target_pairs={{0,1},{1,2},{2,3},{3,4},{4,5},{5,6},{6,7},{7,8},{8,9},{9,10},{10,1... | collective-permute-start | bytes 98312 | tf_op jit(solution)/shard_map/ppermute | solution.py:23
  41.2 4.7 %collective-permute-start.11 = (bf16[128,128]{1,0:T(8,128)(2,1)S(1)}, bf16[128,128]{1,0:T(8,128)(2,1)S(1)}, u32[]{:S(2)}, u32[]{:S(2)}) collective-permute-start(bf16[128,128]{1,0:T(8,128)(2,1)S(1)} %collective-permute-done.10), channel_id=1, source_target_pairs={{1,0},{2,1},{3,2},{4,3},{5,4},{6,5},{7,6},{8,7},{9,8},{10,9},{11,1... | collective-permute-start | bytes 98312 | tf_op jit(solution)/shard_map/ppermute | solution.py:25
  44.2 5.3 %collective-permute-start.26 = (bf16[128,128]{1,0:T(8,128)(2,1)S(1)}, bf16[128,128]{1,0:T(8,128)(2,1)S(1)}, u32[]{:S(2)}, u32[]{:S(2)}) collective-permute-start(bf16[128,128]{1,0:T(8,128)(2,1)S(1)} %collective-permute-done.25), channel_id=1, source_target_pairs={{1,0},{2,1},{3,2},{4,3},{5,4},{6,5},{7,6},{8,7},{9,8},{10,9},{11,1... | collective-permute-start | bytes 98312 | tf_op jit(solution)/shard_map/ppermute | solution.py:25
  44.8 5.3 %collective-permute-start.4 = (bf16[128,128]{1,0:T(8,128)(2,1)S(1)}, bf16[128,128]{1,0:T(8,128)(2,1)S(1)}, u32[]{:S(2)}, u32[]{:S(2)}) collective-permute-start(bf16[128,128]{1,0:T(8,128)(2,1)S(1)} %collective-permute-done.3), channel_id=1, source_target_pairs={{0,1},{1,2},{2,3},{3,4},{4,5},{5,6},{6,7},{7,8},{8,9},{9,10},{10,1... | collective-permute-start | bytes 98312 | tf_op jit(solution)/shard_map/ppermute | solution.py:23
  45.6 4.6 %collective-permute-start.19 = (bf16[128,128]{1,0:T(8,128)(2,1)S(1)}, bf16[128,128]{1,0:T(8,128)(2,1)S(1)}, u32[]{:S(2)}, u32[]{:S(2)}) collective-permute-start(bf16[128,128]{1,0:T(8,128)(2,1)S(1)} %collective-permute-done.18), channel_id=1, source_target_pairs={{0,1},{1,2},{2,3},{3,4},{4,5},{5,6},{6,7},{7,8},{8,9},{9,10},{10,1... | collective-permute-start | bytes 98312 | tf_op jit(solution)/shard_map/ppermute | solution.py:23
  45.9 5.1 %collective-permute-start.12 = (bf16[128,128]{1,0:T(8,128)(2,1)S(1)}, bf16[128,128]{1,0:T(8,128)(2,1)S(1)}, u32[]{:S(2)}, u32[]{:S(2)}) collective-permute-start(bf16[128,128]{1,0:T(8,128)(2,1)S(1)} %collective-permute-done.11), channel_id=1, source_target_pairs={{1,0},{2,1},{3,2},{4,3},{5,4},{6,5},{7,6},{8,7},{9,8},{10,9},{11,1... | collective-permute-start | bytes 98312 | tf_op jit(solution)/shard_map/ppermute | solution.py:25
  49.5 4.6 %collective-permute-start.27 = (bf16[128,128]{1,0:T(8,128)(2,1)S(1)}, bf16[128,128]{1,0:T(8,128)(2,1)S(1)}, u32[]{:S(2)}, u32[]{:S(2)}) collective-permute-start(bf16[128,128]{1,0:T(8,128)(2,1)S(1)} %collective-permute-done.26), channel_id=1, source_target_pairs={{1,0},{2,1},{3,2},{4,3},{5,4},{6,5},{7,6},{8,7},{9,8},{10,9},{11,1... | collective-permute-start | bytes 98312 | tf_op jit(solution)/shard_map/ppermute | solution.py:25
  50.0 4.6 %collective-permute-start.5 = (bf16[128,128]{1,0:T(8,128)(2,1)S(1)}, bf16[128,128]{1,0:T(8,128)(2,1)S(1)}, u32[]{:S(2)}, u32[]{:S(2)}) collective-permute-start(bf16[128,128]{1,0:T(8,128)(2,1)S(1)} %collective-permute-done.4), channel_id=1, source_target_pairs={{0,1},{1,2},{2,3},{3,4},{4,5},{5,6},{6,7},{7,8},{8,9},{9,10},{10,1... | collective-permute-start | bytes 98312 | tf_op jit(solution)/shard_map/ppermute | solution.py:23
  50.2 4.8 %collective-permute-start.20 = (bf16[128,128]{1,0:T(8,128)(2,1)S(1)}, bf16[128,128]{1,0:T(8,128)(2,1)S(1)}, u32[]{:S(2)}, u32[]{:S(2)}) collective-permute-start(bf16[128,128]{1,0:T(8,128)(2,1)S(1)} %collective-permute-done.19), channel_id=1, source_target_pairs={{0,1},{1,2},{2,3},{3,4},{4,5},{5,6},{6,7},{7,8},{8,9},{9,10},{10,1... | collective-permute-start | bytes 98312 | tf_op jit(solution)/shard_map/ppermute | solution.py:23
  55.6 8.6 %collective-permute-start.14 = (bf16[128,128]{1,0:T(8,128)(2,1)S(1)}, bf16[128,128]{1,0:T(8,128)(2,1)S(1)}, u32[]{:S(2)}, u32[]{:S(2)}) collective-permute-start(bf16[128,128]{1,0:T(8,128)(2,1)S(1)} %collective-permute-done.13), channel_id=1, source_target_pairs={{1,0},{2,1},{3,2},{4,3},{5,4},{6,5},{7,6},{8,7},{9,8},{10,9},{11,1... | collective-permute-start | bytes 98312 | tf_op jit(solution)/shard_map/ppermute | solution.py:25
  58.6 36.7 %collective-permute-start.29 = (bf16[128,128]{1,0:T(8,128)(2,1)S(1)}, bf16[128,128]{1,0:T(8,128)(2,1)S(1)}, u32[]{:S(2)}, u32[]{:S(2)}) collective-permute-start(bf16[128,128]{1,0:T(8,128)(2,1)S(1)} %collective-permute-done.28), channel_id=1, source_target_pairs={{1,0},{2,1},{3,2},{4,3},{5,4},{6,5},{7,6},{8,7},{9,8},{10,9},{11,1... | collective-permute-start | bytes 98312 | tf_op jit(solution)/shard_map/ppermute | solution.py:25
  59.1 4.6 %collective-permute-start.7 = (bf16[128,128]{1,0:T(8,128)(2,1)S(1)}, bf16[128,128]{1,0:T(8,128)(2,1)S(1)}, u32[]{:S(2)}, u32[]{:S(2)}) collective-permute-start(bf16[128,128]{1,0:T(8,128)(2,1)S(1)} %collective-permute-done.6), channel_id=1, source_target_pairs={{0,1},{1,2},{2,3},{3,4},{4,5},{5,6},{6,7},{7,8},{8,9},{9,10},{10,1... | collective-permute-start | bytes 98312 | tf_op jit(solution)/shard_map/ppermute | solution.py:23
  59.5 4.6 %collective-permute-start.22 = (bf16[128,128]{1,0:T(8,128)(2,1)S(1)}, bf16[128,128]{1,0:T(8,128)(2,1)S(1)}, u32[]{:S(2)}, u32[]{:S(2)}) collective-permute-start(bf16[128,128]{1,0:T(8,128)(2,1)S(1)} %collective-permute-done.21), channel_id=1, source_target_pairs={{0,1},{1,2},{2,3},{3,4},{4,5},{5,6},{6,7},{7,8},{8,9},{9,10},{10,1... | collective-permute-start | bytes 98312 | tf_op jit(solution)/shard_map/ppermute | solution.py:23
  70.8 19.3 %all-to-all-start.1 = ((bf16[32,2,512]{2,1,0:T(2,128)(2,1)}), bf16[32,2,512]{2,1,0:T(2,128)(2,1)S(1)}, u32[]{:S(2)}, u32[]{:S(2)}) async-start(bf16[32,2,512]{2,1,0:T(2,128)(2,1)} %reshape.397), calls=%async_computation.1 | async-start | bytes 131072 | tf_op jit(solution)/shard_map/all_to_all | solution.py:34
  91.4 14.4 %all-to-all-start.2 = ((bf16[32,16,128]{2,1,0:T(8,128)(2,1)}), bf16[32,16,128]{2,1,0:T(8,128)(2,1)S(1)}, u32[]{:S(2)}, u32[]{:S(2)}) async-start(bf16[32,16,128]{2,1,0:T(8,128)(2,1)} %broadcast_in_dim.10), calls=%async_computation.2 | async-start | bytes 262144 | tf_op jit(solution)/shard_map/all_to_all | solution.py:34
  109.4 13.9 %all-to-all-start.3 = ((bf16[32,2,512]{2,1,0:T(2,128)(2,1)}), bf16[32,2,512]{2,1,0:T(2,128)(2,1)S(1)}, u32[]{:S(2)}, u32[]{:S(2)}) async-start(bf16[32,2,512]{2,1,0:T(2,128)(2,1)} %reshape.399), calls=%async_computation.3 | async-start | bytes 131072 | tf_op jit(solution)/shard_map/all_to_all | solution.py:34
  (18 other events, 54.8 us)
Sparse Core Ops, SparseCore 0:
  10.6 42.7 all-gather.2
  56.0 39.8 all-gather.4
